TPU v7x, 32 devices: a whole 2x2x4 slice. The times are simulated.
32 devices in a mesh: sp: 8 (over z, x), tp: 4 (over y, core).
Axes of the slice: x: 2, y: 2, z: 4, core: 2. Of those that a mesh axis runs over, the one named last changes fastest.
Arguments:
- stream: bfloat16 [1024, 2048], P('sp'), may hold values from -15 to 15
- cotangent: bfloat16 [1024, 2048], P('sp'), may hold values from -6 to 6
- route_ids: int32 [1024, 2], P('sp'), may hold values from 0 to 7, all different within a row; in each aligned block of 128 rows (0 to 127, 128 to 255, ...) at most 64 rows name the same one
- route_weights: float32 [1024, 2], P('sp'), may hold values from 0.1 to 0.9
- w_gate: bfloat16 [8, 2048, 2048], P('sp', None, 'tp'), may hold values from -0.125 to 0.125
- w_up: bfloat16 [8, 2048, 2048], P('sp', None, 'tp'), may hold values from -0.125 to 0.125
- w_down: bfloat16 [8, 2048, 2048], P('sp', 'tp'), may hold values from -0.125 to 0.125
- out_proj: bfloat16 [2048, 512], P(None, 'tp'), may hold values from -0.25 to 0.25
- mixed: bfloat16 [512, 1024], P('tp', 'sp'), may hold values from -6 to 6
- rec_input: bfloat16 [512, 1024], P('tp', 'sp'), may hold values from -6 to 6
- branch_input: bfloat16 [512, 1024], P('tp', 'sp'), may hold values from -6 to 6
- state_before: float32 [512, 1024], P('tp', 'sp'), may hold values from -6 to 6
- rec_gates: bfloat16 [16, 32, 32], P('tp'), may hold values from -1 to 1
- in_gates: bfloat16 [16, 32, 32], P('tp'), may hold values from -1 to 1
- decay_param: float32 [512], P('tp'), may hold values from 4.4 to 11
- decay_shift: float32 [512, 1024], P('tp', 'sp'), may hold values from -1.4 to -1e-05
Outputs:
- grad_gate: bfloat16 [8, 2048, 2048], P('sp', None, 'tp')
- grad_up: bfloat16 [8, 2048, 2048], P('sp', None, 'tp')
- grad_down: bfloat16 [8, 2048, 2048], P('sp', 'tp')
- grad_proj: float32 [2048, 512], P('sp', 'tp')
- grad_rec: float32 [512, 1024], P('tp', 'sp')
- grad_branch: float32 [512, 1024], P('tp', 'sp')
Inputs may be any that keep to these rules, and one draw needn't show every extreme that they name: `route_ids`: each row names 2 different experts; the rows of one device name no expert more than 64 times, a bound that some block reaches on some device.
All inputs are finite; a program needn't handle non-finite values.
Results may differ from a plain program's by a relative error of at most 0.03.
Values may be sent and summed in bfloat16 or wider, within the bound.
A program may use at most 64 MiB of HBM per device.

v0:
```python
import jax
import jax.numpy as jnp
from jax import lax
from jax.sharding import PartitionSpec as P

RATE_SCALE = 8.0
CLAMP_LIMIT = 7.0
GLU_ALPHA = 1.702


def carried_in(part, axis, combine, identity):
    count = lax.axis_size(axis)
    place = lax.axis_index(axis)
    ahead = count - 1 - place
    gathered = jax.tree.map(lambda a: lax.all_gather(a, axis), part)
    state = jax.tree.map(lambda a, e: jnp.zeros_like(a) + jnp.asarray(e, a.dtype), part, identity)

    def one(lap, state):
        source = count - 1 - lap
        return combine(
            state, jax.tree.map(lambda a: lax.dynamic_index_in_dim(a, source, 0, False), gathered)
        )

    return lax.fori_loop(0, ahead, one, state)


def expert_act(gate_pre, up_pre):
    glu_part = jnp.minimum(gate_pre, CLAMP_LIMIT)
    lin_part = jnp.clip(up_pre, -CLAMP_LIMIT, CLAMP_LIMIT)
    return glu_part * jax.nn.sigmoid(GLU_ALPHA * glu_part) * (lin_part + 1.0)


def reverse_step(later_elem, earlier_elem):
    return (later_elem[0] * earlier_elem[0], earlier_elem[1] + earlier_elem[0] * later_elem[1])


def compose_maps(higher_map, lower_map):
    return (lower_map[0] * higher_map[0], lower_map[0] * higher_map[1] + lower_map[1])


def weight_grads(tokens_in, grads_in, d_gate, d_up, act_low):
    g_gate = jnp.einsum("secd,secf->edf", tokens_in, d_gate, preferred_element_type=jnp.float32)
    g_up = jnp.einsum("secd,secf->edf", tokens_in, d_up, preferred_element_type=jnp.float32)
    g_down = jnp.einsum("secf,secd->efd", act_low, grads_in, preferred_element_type=jnp.float32)
    return (g_gate.astype(jnp.bfloat16), g_up.astype(jnp.bfloat16), g_down.astype(jnp.bfloat16))


def local(
    stream,
    cotangent,
    route_ids,
    route_weights,
    w_gate,
    w_up,
    w_down,
    out_proj,
    mixed,
    rec_input,
    branch_input,
    state_before,
    rec_gates,
    in_gates,
    decay_param,
    decay_shift,
):
    sp_count = lax.axis_size("sp")
    tok_rows, model_width = cotangent.shape
    top_count = route_ids.shape[1]
    local_experts = w_gate.shape[0]
    expert_count = local_experts * sp_count
    capacity = 2 * tok_rows * top_count // expert_count
    flat_ids = route_ids.reshape(-1)
    onehot = (flat_ids[:, None] == jnp.arange(expert_count, dtype=jnp.int32)[None, :]).astype(
        jnp.int32
    )
    slot_index = jnp.sum((jnp.cumsum(onehot, axis=0) - onehot) * onehot, axis=1)
    target = flat_ids * capacity + slot_index
    scaled = (route_weights[:, :, None] * cotangent[:, None, :].astype(jnp.float32)).astype(
        jnp.bfloat16
    )
    scaled = scaled.reshape(-1, model_width)
    copies = jnp.broadcast_to(stream[:, None, :], (tok_rows, top_count, model_width)).reshape(
        -1, model_width
    )
    empty_rows = jnp.zeros((expert_count * capacity, model_width), jnp.bfloat16)
    rows_sent = empty_rows.at[target].set(scaled)
    tokens_sent = empty_rows.at[target].set(copies)
    grads_in, tokens_in = (
        lax.all_to_all(rows_sent, "sp", split_axis=0, concat_axis=0, tiled=True),
        lax.all_to_all(tokens_sent, "sp", split_axis=0, concat_axis=0, tiled=True),
    )
    grads_in = grads_in.reshape(sp_count, local_experts, capacity, model_width)
    tokens_in = tokens_in.reshape(sp_count, local_experts, capacity, model_width)
    gate_pre = jnp.einsum("secd,edf->secf", tokens_in, w_gate, preferred_element_type=jnp.float32)
    up_pre = jnp.einsum("secd,edf->secf", tokens_in, w_up, preferred_element_type=jnp.float32)
    act_val, act_vjp = jax.vjp(expert_act, gate_pre, up_pre)
    act_low = act_val.astype(jnp.bfloat16)
    d_act = jnp.einsum("secd,efd->secf", grads_in, w_down, preferred_element_type=jnp.float32)
    d_gate, d_up = act_vjp(d_act)
    d_gate = d_gate.astype(jnp.bfloat16)
    d_up = d_up.astype(jnp.bfloat16)
    grad_gate, grad_up, grad_down = weight_grads(tokens_in, grads_in, d_gate, d_up, act_low)
    partial_value = jnp.einsum("secf,edf->secd", d_gate, w_gate, preferred_element_type=jnp.float32)
    partial_value = partial_value + jnp.einsum(
        "secf,edf->secd", d_up, w_up, preferred_element_type=jnp.float32
    )
    share = lax.psum_scatter(
        partial_value.astype(jnp.bfloat16), "tp", scatter_dimension=3, tiled=True
    )
    share_cols = share.shape[3]
    returned = lax.all_to_all(
        share.reshape(-1, share_cols), "sp", split_axis=0, concat_axis=0, tiled=True
    )
    per_pair = returned[target].astype(jnp.float32).reshape(tok_rows, top_count, share_cols)
    own_cols = lax.dynamic_slice_in_dim(cotangent, lax.axis_index("tp") * share_cols, share_cols, 1)
    share_low = (own_cols.astype(jnp.float32) + jnp.sum(per_pair, axis=1)).astype(jnp.bfloat16)
    stream_low = lax.all_gather(share_low, "tp", axis=1, tiled=True)
    d_mixed = lax.dot_general(
        out_proj, stream_low, (((0,), (1,)), ((), ())), preferred_element_type=jnp.float32
    )
    grad_proj = lax.psum_scatter(
        lax.dot_general(
            stream_low, mixed, (((0,), (1,)), ((), ())), preferred_element_type=jnp.float32
        ).astype(jnp.bfloat16),
        "sp",
        scatter_dimension=0,
        tiled=True,
    ).astype(jnp.float32)
    channels, positions = rec_input.shape
    gate_heads = rec_gates.shape[0]
    head_dim = rec_gates.shape[1]
    rec_heads = rec_input.reshape(gate_heads, head_dim, positions)
    rec_pre = jnp.einsum(
        "hij,hit->hjt", rec_gates, rec_heads, preferred_element_type=jnp.float32
    ).reshape(channels, positions)
    in_pre = jnp.einsum(
        "hij,hit->hjt", in_gates, rec_heads, preferred_element_type=jnp.float32
    ).reshape(channels, positions)
    rec_gate = jax.nn.sigmoid(rec_pre)
    in_gate = jax.nn.sigmoid(in_pre)
    soft_plus = jax.nn.softplus(-decay_param)[:, None]
    log_decay = -RATE_SCALE * rec_gate * soft_plus + decay_shift
    decay_rate = jnp.exp(log_decay)
    token_position = lax.axis_index("sp") * positions + jnp.arange(positions, dtype=jnp.int32)
    at_start = (token_position == 0)[None, :]
    raw_mult = jnp.sqrt(-jnp.expm1(2.0 * log_decay))
    multiplier = jnp.where(at_start, 1.0, raw_mult)
    rec_value = rec_input.astype(jnp.float32)
    state_now = decay_rate * state_before + multiplier * in_gate * rec_value
    gelu_val, gelu_vjp = jax.vjp(jax.nn.gelu, branch_input.astype(jnp.float32))
    grad_branch = gelu_vjp(d_mixed * state_now)[0]
    d_state = d_mixed * gelu_val
    next_decay = jnp.concatenate([decay_rate[:, 1:], jnp.zeros((channels, 1), jnp.float32)], axis=1)
    local_adj = lax.associative_scan(reverse_step, (next_decay, d_state), reverse=True, axis=1)[1]
    log_cumsum = jnp.cumsum(log_decay, axis=1)
    total_log = log_cumsum[:, -1:]
    tail_decay = jnp.exp(total_log - log_cumsum)
    device_prod = jnp.exp(total_log[:, 0])
    head_term = decay_rate[:, 0] * local_adj[:, 0]
    identity = (jnp.ones((channels,), jnp.float32), jnp.zeros((channels,), jnp.float32))
    carried = carried_in((device_prod, head_term), "sp", compose_maps, identity)
    adjoint = local_adj + tail_decay * carried[1][:, None]
    mult_term = adjoint * in_gate * rec_value * decay_rate * decay_rate / raw_mult
    d_log = adjoint * state_before * decay_rate - jnp.where(at_start, 0.0, mult_term)
    d_rec_pre = (d_log * -RATE_SCALE * soft_plus * rec_gate * (1.0 - rec_gate)).astype(jnp.bfloat16)
    d_in_pre = (adjoint * multiplier * rec_value * in_gate * (1.0 - in_gate)).astype(jnp.bfloat16)
    back_rec = jnp.einsum(
        "hij,hjt->hit",
        rec_gates,
        d_rec_pre.reshape(gate_heads, head_dim, positions),
        preferred_element_type=jnp.float32,
    )
    back_in = jnp.einsum(
        "hij,hjt->hit",
        in_gates,
        d_in_pre.reshape(gate_heads, head_dim, positions),
        preferred_element_type=jnp.float32,
    )
    grad_rec = adjoint * multiplier * in_gate + (back_rec + back_in).reshape(channels, positions)
    return (grad_gate, grad_up, grad_down, grad_proj, grad_rec, grad_branch)


def solution(mesh):
    placed = (
        P("sp", None),
        P("sp", None),
        P("sp", None),
        P("sp", None),
        P("sp", None, "tp"),
        P("sp", None, "tp"),
        P("sp", "tp", None),
        P(None, "tp"),
        P("tp", "sp"),
        P("tp", "sp"),
        P("tp", "sp"),
        P("tp", "sp"),
        P("tp", None, None),
        P("tp", None, None),
        P("tp"),
        P("tp", "sp"),
    )
    return jax.shard_map(
        local,
        mesh=mesh,
        in_specs=placed,
        out_specs=(
            P("sp", None, "tp"),
            P("sp", None, "tp"),
            P("sp", "tp", None),
            P("sp", "tp"),
            P("tp", "sp"),
            P("tp", "sp"),
        ),
        check_vma=False,
    )
```

profile of v0, /device:TPU:0, one launch (start us, length us, event | category | flops | bytes accessed | tf_op | source)
XLA Modules:
  0.0 267.8 jit_solution(8226103866001131693)
XLA Ops:
  7.2 0.8 broadcast_multiply_fusion
  8.0 0.8 copy.37
  10.2 1.7 broadcast_in_dim.17
  11.9 1.2 reshape.255
  13.2 4.4 %scatter_custom_fusion = bf16[512,2048]{1,0:T(8,128)(2,1)} fusion(s32[256]{0:T(256)S(1)} %bitcast.195, bf16[256,2048]{1,0:T(8,128)(2,1)} %reshape.255, bf16[]{:T(256)} %constant.45.clone.1), kind=kCustom, calls=%fused_computation.58 | custom fusion | bytes 2097664 | tf_op jit(solution)/shard_map/scatter | solution.py:87
  17.6 7.4 %all-to-all-start = ((bf16[8,64,2048]{2,1,0:T(8,128)(2,1)}), bf16[8,64,2048]{2,1,0:T(8,128)(2,1)}, u32[]{:S(2)}, u32[]{:S(2)}) async-start(bf16[8,64,2048]{2,1,0:T(8,128)(2,1)} %bitcast.184), calls=%async_computation | async-start | bytes 4194304 | tf_op jit(solution)/shard_map/all_to_all | solution.py:90
  25.0 2.4 mul.301
  27.4 3.7 %mul.302 = f32[256,2048]{1,0:T(8,128)} reshape(f32[128,2,2048]{2,1,0:T(2,128)} %mul.301) | data formatting | bytes 4194304 | tf_op jit(solution)/shard_map/mul | solution.py:78
  31.3 4.8 %scatter_custom_fusion.1 = bf16[512,2048]{1,0:T(8,128)(2,1)} fusion(s32[256]{0:T(256)S(1)} %bitcast.196, f32[256,2048]{1,0:T(8,128)} %mul.302, f32[256]{0:T(256)S(1)} %mul.299, bf16[]{:T(256)} %constant.45.clone.1), kind=kCustom, calls=%fused_computation.41 | custom fusion | flops 1048576 | bytes 4195330 | tf_op jit(solution)/shard_map/scatter | solution.py:86
  36.1 37.2 %all-to-all-done = bf16[8,64,2048]{2,1,0:T(8,128)(2,1)} async-done(((bf16[8,64,2048]{2,1,0:T(8,128)(2,1)}), bf16[8,64,2048]{2,1,0:T(8,128)(2,1)}, u32[]{:S(2)}, u32[]{:S(2)}) %all-to-all-start) | async-done | bytes 2097184 | tf_op jit(solution)/shard_map/all_to_all | solution.py:90
  73.4 4.3 %all-to-all-start.1 = ((bf16[8,64,2048]{2,1,0:T(8,128)(2,1)}), bf16[8,64,2048]{2,1,0:T(8,128)(2,1)}, u32[]{:S(2)}, u32[]{:S(2)}) async-start(bf16[8,64,2048]{2,1,0:T(8,128)(2,1)} %bitcast.183), calls=%async_computation.1 | async-start | bytes 4194304 | tf_op jit(solution)/shard_map/all_to_all | solution.py:89
  77.9 4.4 %fusion.9 = f32[8,64,512]{2,1,0:T(8,128)} fusion(bf16[8,64,2048]{2,1,0:T(8,128)(2,1)} %all-to-all-done, bf16[1,2048,512]{2,1,0:T(8,128)(2,1)} %param.23), kind=kOutput, calls=%fused_computation.19 | convolution fusion | flops 1073741824 | bytes 5242880 | tf_op jit(solution)/shard_map/secd,edf->secf/dot_general | solution.py:95
  82.4 3.8 %fusion.6 = f32[8,64,512]{2,1,0:T(8,128)} fusion(bf16[8,64,2048]{2,1,0:T(8,128)(2,1)} %all-to-all-done, bf16[1,2048,512]{2,1,0:T(8,128)(2,1)S(1)} %copy-done), kind=kOutput, calls=%fused_computation.16 | convolution fusion | flops 1073741824 | bytes 5242880 | tf_op jit(solution)/shard_map/secd,edf->secf/dot_general | solution.py:94
  86.2 39.3 %all-to-all-done.1 = bf16[8,64,2048]{2,1,0:T(8,128)(2,1)} async-done(((bf16[8,64,2048]{2,1,0:T(8,128)(2,1)}), bf16[8,64,2048]{2,1,0:T(8,128)(2,1)}, u32[]{:S(2)}, u32[]{:S(2)}) %all-to-all-start.1) | async-done | bytes 2097184 | tf_op jit(solution)/shard_map/all_to_all | solution.py:89
  125.5 5.1 %fusion.28 = (bf16[8,1,64,512]{3,2,0,1:T(8,128)(2,1)S(1)}, bf16[8,1,64,512]{3,2,0,1:T(8,128)(2,1)S(1)}) fusion(f32[8,64,512]{2,1,0:T(8,128)} %fusion.9, f32[8,64,512]{2,1,0:T(8,128)} %fusion.6, bf16[8,64,2048]{2,1,0:T(8,128)(2,1)} %all-to-all-done.1, bf16[1,512,2048]{2,1,0:T(8,128)(2,1)} %param.24), kind=kOutput, calls=%fused_computation.43 | convolution fusion | flops 1082916864 | bytes 7340032 | tf_op jit(solution)/shard_map/secd,efd->secf/dot_general | solution.py:98
  130.6 1.3 fusion.4
  132.4 2.6 fusion
  138.4 1.0 fusion.21
  140.1 4.4 %fusion.1 = bf16[1,2048,512]{2,1,0:T(8,128)(2,1)} fusion(bf16[8,64,2048]{2,1,0:T(8,128)(2,1)} %all-to-all-done, bf16[8,1,64,512]{3,2,0,1:T(8,128)(2,1)S(1)} %get-tuple-element.118), kind=kOutput, calls=%fused_computation.10 | convolution fusion | flops 1074790400 | bytes 4718592 | tf_op jit(solution)/shard_map/secd,secf->edf/dot_general | solution.py:42
  144.5 21.0 %reduce-scatter.3.cloned.1.call-done = bf16[8,1,64,512]{3,2,0,1:T(8,128)(2,1)} async-done(((bf16[8,1,64,2048]{3,2,0,1:T(8,128)(2,1)}), bf16[8,1,64,512]{3,2,0,1:T(8,128)(2,1)}) %reduce-scatter.3.cloned.1.call-update) | async-done | bytes 524304 | tf_op jit(solution)/shard_map/reduce_scatter | solution.py:107
  165.4 5.5 %all-to-all-start.2 = ((bf16[8,64,512]{2,1,0:T(8,128)(2,1)}), bf16[8,64,512]{2,1,0:T(8,128)(2,1)S(1)}, u32[]{:S(2)}, u32[]{:S(2)}) async-start(bf16[8,64,512]{2,1,0:T(8,128)(2,1)} %bitcast.185), calls=%async_computation.3 | async-start | bytes 1048576 | tf_op jit(solution)/shard_map/all_to_all | solution.py:111
  171.0 4.4 %fusion.2 = bf16[1,2048,512]{2,1,0:T(8,128)(2,1)} fusion(bf16[8,64,2048]{2,1,0:T(8,128)(2,1)} %all-to-all-done, bf16[8,1,64,512]{3,2,0,1:T(8,128)(2,1)} %copy-done.4), kind=kOutput, calls=%fused_computation.11 | convolution fusion | flops 1074790400 | bytes 4718592 | tf_op jit(solution)/shard_map/secd,secf->edf/dot_general | solution.py:43
  175.4 4.4 %fusion.3 = bf16[1,512,2048]{2,1,0:T(8,128)(2,1)} fusion(bf16[8,64,2048]{2,1,0:T(8,128)(2,1)} %all-to-all-done.1, f32[8,64,512]{2,1,0:T(8,128)S(1)} %copy-done.16, f32[8,64,512]{2,1,0:T(8,128)S(1)} %copy-done.17), kind=kOutput, calls=%fused_computation.12 | convolution fusion | flops 1077411840 | bytes 6291456 | tf_op jit(solution)/shard_map/secf,secd->efd/dot_general | solution.py:44
  179.8 5.5 %all-to-all-done.2 = bf16[8,64,512]{2,1,0:T(8,128)(2,1)S(1)} async-done(((bf16[8,64,512]{2,1,0:T(8,128)(2,1)}), bf16[8,64,512]{2,1,0:T(8,128)(2,1)S(1)}, u32[]{:S(2)}, u32[]{:S(2)}) %all-to-all-start.2) | async-done | bytes 524320 | tf_op jit(solution)/shard_map/all_to_all | solution.py:111
  185.3 1.2 gather_fusion
  187.4 6.7 %all_gather.11 = bf16[128,2048]{1,0:T(8,128)(2,1)S(1)} all-gather(bf16[128,512]{1,0:T(8,128)(2,1)S(1)} %add_convert_fusion.1), channel_id=1, replica_groups=mesh['sp'=8,'tp'=4] {'tp'}, dimensions={1}, use_global_device_ids=true | all-gather | bytes 655360 | tf_op jit(solution)/shard_map/all_gather | solution.py:117
  194.2 1.4 fusion.49
  196.7 1.1 convolution_convert_fusion
  198.3 19.0 %all-gather = f32[1024,1]{0,1:T(1,128)S(1)} all-gather(f32[128,1]{0,1:T(1,128)S(1)} %get-tuple-element.122), channel_id=2, replica_groups=mesh['sp'=8,'tp'=4] {'sp'}, dimensions={0}, use_global_device_ids=true | all-gather | bytes 4608 | tf_op jit(solution)/shard_map/all_gather | solution.py:15
  217.3 16.3 %all-gather.1 = f32[1024,1]{0,1:T(1,128)S(1)} all-gather(f32[128,1]{0,1:T(1,128)S(1)} %add_multiply_fusion.3), channel_id=3, replica_groups=mesh['sp'=8,'tp'=4] {'sp'}, dimensions={0}, use_global_device_ids=true | all-gather | bytes 4608 | tf_op jit(solution)/shard_map/all_gather | solution.py:15
  236.1 23.4 %reduce-scatter.5.cloned.1.call-done = bf16[256,128]{1,0:T(8,128)(2,1)} async-done(((bf16[2048,128]{1,0:T(8,128)(2,1)}), bf16[256,128]{1,0:T(8,128)(2,1)}) %reduce-scatter.5.cloned.1.call-update) | async-done | bytes 65552 | tf_op jit(solution)/shard_map/reduce_scatter | solution.py:121
  259.5 1.5 convert_element_type.107
  (174 shorter events, 11.2 us)
Async XLA Ops:
  7.2 75.2 %copy-start = (bf16[1,2048,512]{2,1,0:T(8,128)(2,1)S(1)}, bf16[1,2048,512]{2,1,0:T(8,128)(2,1)}, u32[]{:S(2)}) copy-start(bf16[1,2048,512]{2,1,0:T(8,128)(2,1)} %param.22) | copy-start | bytes 6291460
  17.6 7.4 %copy-start.2 = (bf16[128,2048]{1,0:T(8,128)(2,1)S(1)}, bf16[128,2048]{1,0:T(8,128)(2,1)}, u32[]{:S(2)}) copy-start(bf16[128,2048]{1,0:T(8,128)(2,1)} %param.19) | copy-start | bytes 1572868
  17.6 55.8 %all-to-all-start = ((bf16[8,64,2048]{2,1,0:T(8,128)(2,1)}), bf16[8,64,2048]{2,1,0:T(8,128)(2,1)}, u32[]{:S(2)}, u32[]{:S(2)}) async-start(bf16[8,64,2048]{2,1,0:T(8,128)(2,1)} %bitcast.184), calls=%async_computation | async-start | bytes 4194304 | tf_op jit(solution)/shard_map/all_to_all | solution.py:90
  27.4 3.7 %copy-start.14 = (f32[128,2]{0,1:T(2,128)S(1)}, f32[128,2]{0,1:T(2,128)}, u32[]{:S(2)}) copy-start(f32[128,2]{0,1:T(2,128)} %param.21) | copy-start | bytes 3076
  73.4 52.2 %all-to-all-start.1 = ((bf16[8,64,2048]{2,1,0:T(8,128)(2,1)}), bf16[8,64,2048]{2,1,0:T(8,128)(2,1)}, u32[]{:S(2)}, u32[]{:S(2)}) async-start(bf16[8,64,2048]{2,1,0:T(8,128)(2,1)} %bitcast.183), calls=%async_computation.1 | async-start | bytes 4194304 | tf_op jit(solution)/shard_map/all_to_all | solution.py:89
  77.7 87.7 %reduce-scatter.3.cloned.1.call-start = ((), (), s32[]{:S(2)}) async-start(), calls=%async_computation.5 | async-start | bytes 2621440 | tf_op jit(solution)/shard_map/reduce_scatter | solution.py:107
  130.6 1.3 copy-start.4
  130.6 1.8 copy-start.1
  135.0 0.8 copy-start.10
  135.0 1.5 copy-start.12
  135.0 1.8 copy-start.9
  135.0 2.5 copy-start.6
  135.0 2.6 copy-start.7
  135.0 5.1 %copy-start.15 = (f32[128]{0:T(128)S(1)}, f32[128]{0:T(128)}, u32[]{:S(2)}) copy-start(f32[128]{0:T(128)} %param.32) | copy-start | bytes 1540
  165.4 19.8 %all-to-all-start.2 = ((bf16[8,64,512]{2,1,0:T(8,128)(2,1)}), bf16[8,64,512]{2,1,0:T(8,128)(2,1)S(1)}, u32[]{:S(2)}, u32[]{:S(2)}) async-start(bf16[8,64,512]{2,1,0:T(8,128)(2,1)} %bitcast.185), calls=%async_computation.3 | async-start | bytes 1048576 | tf_op jit(solution)/shard_map/all_to_all | solution.py:111
  170.9 88.5 %reduce-scatter.5.cloned.1.call-start = ((), (), s32[]{:S(2)}) async-start(), calls=%async_computation.6 | async-start | bytes 589824 | tf_op jit(solution)/shard_map/reduce_scatter | solution.py:121
  171.0 4.5 %copy-start.16 = (f32[8,64,512]{2,1,0:T(8,128)S(1)}, f32[8,64,512]{2,1,0:T(8,128)}, u32[]{:S(2)}) copy-start(f32[8,64,512]{2,1,0:T(8,128)} %fusion.9) | copy-start | bytes 3145732
  171.0 4.4 %copy-start.17 = (f32[8,64,512]{2,1,0:T(8,128)S(1)}, f32[8,64,512]{2,1,0:T(8,128)}, u32[]{:S(2)}) copy-start(f32[8,64,512]{2,1,0:T(8,128)} %fusion.6) | copy-start | bytes 3145732
  187.4 9.3 %copy-start.8 = (bf16[128,128]{1,0:T(8,128)(2,1)S(1)}, bf16[128,128]{1,0:T(8,128)(2,1)}, u32[]{:S(2)}) copy-start(bf16[128,128]{1,0:T(8,128)(2,1)} %param.26) | copy-start | bytes 98308
  195.8 38.0 %copy-start.3 = (f32[128,128]{0,1:T(8,128)S(1)}, f32[128,128]{0,1:T(8,128)}, u32[]{:S(2)}) copy-start(f32[128,128]{0,1:T(8,128)} %copy.42) | copy-start | bytes 196612
  195.9 38.0 %copy-start.5 = (bf16[128,128]{0,1:T(8,128)(2,1)S(1)}, bf16[128,128]{0,1:T(8,128)(2,1)}, u32[]{:S(2)}) copy-start(bf16[128,128]{0,1:T(8,128)(2,1)} %copy.48) | copy-start | bytes 98308
  196.5 37.8 %copy-start.11 = (bf16[4,32,32]{2,1,0:T(8,128)(2,1)S(1)}, bf16[4,32,32]{2,1,0:T(8,128)(2,1)}, u32[]{:S(2)}) copy-start(bf16[4,32,32]{2,1,0:T(8,128)(2,1)} %param.30) | copy-start | bytes 24580
  196.7 37.7 %copy-start.13 = (bf16[4,32,32]{2,1,0:T(8,128)(2,1)S(1)}, bf16[4,32,32]{2,1,0:T(8,128)(2,1)}, u32[]{:S(2)}) copy-start(bf16[4,32,32]{2,1,0:T(8,128)(2,1)} %param.31) | copy-start | bytes 24580
Sparse Core Ops, SparseCore 0:
  135.2 30.2 reduce-scatter.2
  198.0 61.4 reduce-scatter.4
where the time goes:
time: 269 us; the launch traced here: 268 us
  waiting for transfers between devices  126 us (47%)
  blocking collectives  42 us (16%)
  matrix products  34.4 us (13%)
  local copies, waits for them, and re-layouts  23.5 us (9%)
  starting transfers between devices  17.5 us (7%)
  between operations  14.8 us (6%)
  other arithmetic  9.23 us (3%)
    all_to_all x1, waiting for transfers between devices, local(): lax.all_to_all(rows_sent, 'sp', split_axis=0, concat_axis=0, tiled=True)  39.3 us
    all_to_all x1, waiting for transfers between devices, local(): lax.all_to_all(tokens_sent, 'sp', split_axis=0, concat_axis=0, tiled=True)  37.2 us
    all_gather x2, blocking collectives, carried_in(): gathered = jax.tree.map(lambda a: lax.all_gather(a, axis), part)  35.3 us
    reduce_scatter x1, waiting for transfers between devices, local(): lax.psum_scatter(lax.dot_general(stream_low, mixed, (((0,), (1,)), ((), (...  23.4 us
    reduce_scatter x1, waiting for transfers between devices, local(): lax.psum_scatter(partial_value.astype(jnp.bfloat16), 'tp', scatter_dimens...  21 us
    all_to_all x1, starting transfers between devices, local(): lax.all_to_all(tokens_sent, 'sp', split_axis=0, concat_axis=0, tiled=True)  7.41 us
    all_gather x1, blocking collectives, local(): stream_low = lax.all_gather(share_low, 'tp', axis=1, tiled=True)  6.72 us
    mul x3, local copies, waits for them, and re-layouts, local(): route_weights[:, :, None] * cotangent[:, None, :].astype(jnp.float32)  6.17 us
  transfers between devices with their start and end apart: 5, of which 5 were waited for; matrix products, arithmetic and copies ran while one was open for 15% of the time, Pallas kernels for 0%

commit v1 on v0

--- a/solution.py
+++ b/solution.py
@@ -1,27 +1,18 @@
+import functools
+
 import jax
 import jax.numpy as jnp
 from jax import lax
+from jax.experimental import pallas as pl
+from jax.experimental.pallas import tpu as pltpu
 from jax.sharding import PartitionSpec as P
 
 RATE_SCALE = 8.0
 CLAMP_LIMIT = 7.0
 GLU_ALPHA = 1.702
-
-
-def carried_in(part, axis, combine, identity):
-    count = lax.axis_size(axis)
-    place = lax.axis_index(axis)
-    ahead = count - 1 - place
-    gathered = jax.tree.map(lambda a: lax.all_gather(a, axis), part)
-    state = jax.tree.map(lambda a, e: jnp.zeros_like(a) + jnp.asarray(e, a.dtype), part, identity)
-
-    def one(lap, state):
-        source = count - 1 - lap
-        return combine(
-            state, jax.tree.map(lambda a: lax.dynamic_index_in_dim(a, source, 0, False), gathered)
-        )
-
-    return lax.fori_loop(0, ahead, one, state)
+CORES = 2
+MESH = pl.DeviceIdType.MESH
+VMEM_LIMIT = 60 * 1024 * 1024
 
 
 def expert_act(gate_pre, up_pre):
@@ -32,10 +23,6 @@
 
 def reverse_step(later_elem, earlier_elem):
     return (later_elem[0] * earlier_elem[0], earlier_elem[1] + earlier_elem[0] * later_elem[1])
-
-
-def compose_maps(higher_map, lower_map):
-    return (lower_map[0] * higher_map[0], lower_map[0] * higher_map[1] + lower_map[1])
 
 
 def weight_grads(tokens_in, grads_in, d_gate, d_up, act_low):
@@ -43,6 +30,446 @@
     g_up = jnp.einsum("secd,secf->edf", tokens_in, d_up, preferred_element_type=jnp.float32)
     g_down = jnp.einsum("secf,secd->efd", act_low, grads_in, preferred_element_type=jnp.float32)
     return (g_gate.astype(jnp.bfloat16), g_up.astype(jnp.bfloat16), g_down.astype(jnp.bfloat16))
+
+
+def aligned(value, size):
+    return pl.multiple_of(value * size, size)
+
+
+def remote(src, dst, send_sem, recv_sem, device):
+    return pltpu.make_async_remote_copy(
+        src_ref=src,
+        dst_ref=dst,
+        send_sem=send_sem,
+        recv_sem=recv_sem,
+        device_id=device,
+        device_id_type=MESH,
+    )
+
+
+class Place:
+    def __init__(self, n_sp, n_tp):
+        self.n, self.ny = n_sp, n_tp // CORES
+        self.s, self.t = lax.axis_index("sp"), lax.axis_index("tp")
+        self.y, self.c = self.t // CORES, lax.rem(self.t, CORES)
+        self.partner = (self.s, self.y * CORES + 1 - self.c)
+
+    def sp_peer(self, i):
+        return lax.rem(self.s + i, self.n)
+
+    def sp_source(self, i):
+        return lax.rem(self.s + self.n - i, self.n)
+
+    def y_peer(self, j):
+        return lax.rem(self.y + j, self.ny)
+
+    def y_source(self, j):
+        return lax.rem(self.y + self.ny - j, self.ny)
+
+    def tp_of(self, y, c):
+        return y * CORES + c
+
+    def barrier(self, along_tp=True):
+        sem = pltpu.get_barrier_semaphore()
+
+        def greet(device):
+            pl.semaphore_signal(sem, inc=1, device_id=device, device_id_type=MESH)
+
+        for i in range(1, self.n):
+            greet((self.sp_peer(i), self.t))
+        count = self.n - 1
+        if along_tp:
+            for j in range(1, self.ny):
+                greet((self.s, self.tp_of(self.y_peer(j), self.c)))
+            greet(self.partner)
+            count += self.ny
+        pl.semaphore_wait(sem, count)
+
+
+def dispatch_kernel(
+    n_sp, n_tp, tok_src, grd_src, tok_out, grd_out, own_sem, sa, ra, sy, ry, sc, rc
+):
+    at = Place(n_sp, n_tp)
+    rows = tok_src.shape[0] // n_sp
+    cols = tok_src.shape[1]
+    pairs = ((tok_src, tok_out), (grd_src, grd_out))
+
+    def block(out, source, tp):
+        return out.at[pl.ds(aligned(source, rows), rows), pl.ds(aligned(tp, cols), cols)]
+
+    def first(a, i):
+        src, out = pairs[a]
+        peer = at.sp_peer(i)
+        return remote(
+            src.at[pl.ds(aligned(peer, rows), rows), :],
+            block(out, at.s, at.t),
+            sa.at[a, i],
+            ra.at[a, i],
+            (peer, at.t),
+        )
+
+    def along_y(a, i, j, source, outgoing):
+        src, out = pairs[a]
+        tp = at.t if outgoing else at.tp_of(at.y_source(j), at.c)
+        spot = block(out, source, tp)
+        return remote(
+            spot, spot, sy.at[a, i, j], ry.at[a, i, j], (at.s, at.tp_of(at.y_peer(j), at.c))
+        )
+
+    def across(a, i, j, source, outgoing):
+        src, out = pairs[a]
+        tp = at.tp_of(at.y_source(j), at.c if outgoing else 1 - at.c)
+        spot = block(out, source, tp)
+        return remote(spot, spot, sc.at[a, i, j], rc.at[a, i, j], at.partner)
+
+    own = []
+    for a in range(2):
+        src, out = pairs[a]
+        copy = pltpu.make_async_copy(
+            src.at[pl.ds(aligned(at.s, rows), rows), :], block(out, at.s, at.t), own_sem.at[a]
+        )
+        copy.start()
+        own.append(copy)
+    at.barrier()
+
+    for a in range(2):
+
+        def send(i, _):
+            first(a, i).start()
+            return 0
+
+        lax.fori_loop(1, n_sp, send, 0)
+    for copy in own:
+        copy.wait()
+
+    def pass_on(a, i):
+        source = at.sp_source(i)
+        for j in range(1, at.ny):
+            along_y(a, i, j, source, True).start()
+        across(a, i, 0, source, True).start()
+
+    def relay(a, i):
+        source = at.sp_source(i)
+        for j in range(1, at.ny):
+            along_y(a, i, j, source, False).wait_recv()
+            across(a, i, j, source, True).start()
+
+    for a in range(2):
+        pass_on(a, 0)
+    for a in range(2):
+
+        def step(i, _):
+            first(a, i).wait_recv()
+            pass_on(a, i)
+            relay(a, i - 1)
+            return 0
+
+        lax.fori_loop(1, n_sp, step, 0)
+        relay(a, n_sp - 1)
+
+    for a in range(2):
+
+        def drain(i, _):
+            source = at.sp_source(i)
+            for j in range(at.ny):
+                across(a, i, j, source, False).wait_recv()
+                across(a, i, j, source, True).wait_send()
+            for j in range(1, at.ny):
+                along_y(a, i, j, source, True).wait_send()
+            return 0
+
+        def drain_first(i, _):
+            first(a, i).wait_send()
+            return 0
+
+        lax.fori_loop(0, n_sp, drain, 0)
+        lax.fori_loop(1, n_sp, drain_first, 0)
+
+
+def dispatch(tok_src, grd_src, n_sp, n_tp):
+    total, cols = tok_src.shape
+    ny = n_tp // CORES
+    dma = pltpu.SemaphoreType.DMA
+    shape = jax.ShapeDtypeStruct((total, cols * n_tp), jnp.bfloat16)
+    return pl.pallas_call(
+        functools.partial(dispatch_kernel, n_sp, n_tp),
+        out_shape=(shape, shape),
+        in_specs=[pl.BlockSpec(memory_space=pltpu.VMEM)] * 2,
+        out_specs=[pl.BlockSpec(memory_space=pl.ANY)] * 2,
+        scratch_shapes=[
+            dma((2,)),
+            dma((2, n_sp)),
+            dma((2, n_sp)),
+            dma((2, n_sp, ny)),
+            dma((2, n_sp, ny)),
+            dma((2, n_sp, ny)),
+            dma((2, n_sp, ny)),
+        ],
+        compiler_params=pltpu.CompilerParams(
+            collective_id=0, has_side_effects=True, vmem_limit_bytes=VMEM_LIMIT
+        ),
+    )(tok_src, grd_src)
+
+
+def return_kernel(
+    n_sp, n_tp, part, pick, cot, out,
+    core_in, own_sum, y_out, y_in, ret_out, ret_in, low,
+    sc, rc, sy, ry, sr, rr, sl, rl, sp_, rp_, own_sem,
+):
+    at = Place(n_sp, n_tp)
+    rows = part.shape[0] // n_sp
+    cols = part.shape[1] // n_tp
+    tok = cot.shape[0]
+
+    def piece(peer, tp):
+        return pl.ds(aligned(peer, rows), rows), pl.ds(aligned(tp, cols), cols)
+
+    def peer_of(i):
+        return at.sp_peer(i + 1)
+
+    def core_copy(i, j):
+        r, c = piece(peer_of(i), at.tp_of(at.y_peer(j), 1 - at.c))
+        return remote(part.at[r, c], core_in.at[i, j], sc.at[i, j], rc.at[i, j], at.partner)
+
+    def y_copy(i, j):
+        return remote(
+            y_out.at[i, j],
+            y_in.at[i, j],
+            sy.at[i, j],
+            ry.at[i, j],
+            (at.s, at.tp_of(at.y_peer(j), at.c)),
+        )
+
+    def home_copy(i):
+        return remote(
+            ret_out.at[i],
+            ret_in.at[pl.ds(aligned(at.s, rows), rows), :],
+            sr.at[i],
+            rr.at[i],
+            (peer_of(i), at.t),
+        )
+
+    at.barrier()
+
+    def send_core(i, _):
+        for j in range(at.ny):
+            core_copy(i, j).start()
+        return 0
+
+    lax.fori_loop(0, n_sp, send_core, 0)
+
+    def reduce_core(i):
+        peer = peer_of(i)
+        for j in list(range(1, at.ny)) + [0]:
+            core_copy(i, j).wait_recv()
+            r, c = piece(peer, at.tp_of(at.y_peer(j), at.c))
+            both = part[r, c].astype(jnp.float32) + core_in[i, j].astype(jnp.float32)
+            if j:
+                y_out[i, j] = both.astype(jnp.bfloat16)
+                y_copy(i, j).start()
+            else:
+                own_sum[i] = both
+
+    def reduce_y(i):
+        total = own_sum[i]
+        for j in range(1, at.ny):
+            y_copy(i, j).wait_recv()
+            total = total + y_in[i, j].astype(jnp.float32)
+        return total.astype(jnp.bfloat16)
+
+    def send_home(i):
+        ret_out[i] = reduce_y(i)
+        home_copy(i).start()
+
+    reduce_core(0)
+
+    def step(i, _):
+        reduce_core(i)
+        send_home(i - 1)
+        return 0
+
+    lax.fori_loop(1, n_sp, step, 0)
+    ret_in[pl.ds(aligned(at.s, rows), rows), :] = reduce_y(n_sp - 1)
+
+    def wait_home(i, _):
+        source = at.sp_source(i + 1)
+        spot = ret_in.at[pl.ds(aligned(source, rows), rows), :]
+        remote(ret_out.at[i], spot, sr.at[i], rr.at[i], (peer_of(i), at.t)).wait_recv()
+        return 0
+
+    lax.fori_loop(0, n_sp - 1, wait_home, 0)
+    own_cols = cot[:, pl.ds(aligned(at.t, cols), cols)].astype(jnp.float32)
+    pair_sum = jnp.dot(pick[...], ret_in[...], preferred_element_type=jnp.float32)
+    low[...] = (own_cols + pair_sum).astype(jnp.bfloat16)
+
+    def spot_of(tp):
+        return out.at[:, pl.ds(aligned(tp, cols), cols)]
+
+    def low_y(j):
+        return remote(
+            low, spot_of(at.t), sl.at[j], rl.at[j], (at.s, at.tp_of(at.y_peer(j), at.c))
+        )
+
+    def low_y_in(j):
+        return remote(
+            low,
+            spot_of(at.tp_of(at.y_source(j), at.c)),
+            sl.at[j],
+            rl.at[j],
+            (at.s, at.tp_of(at.y_peer(j), at.c)),
+        )
+
+    def low_core(j, outgoing):
+        spot = spot_of(at.tp_of(at.y_source(j), at.c if outgoing else 1 - at.c))
+        src = low if j == 0 else spot
+        return remote(src, spot, sp_.at[j], rp_.at[j], at.partner)
+
+    for j in range(1, at.ny):
+        low_y(j).start()
+    low_core(0, True).start()
+    own = pltpu.make_async_copy(low, spot_of(at.t), own_sem)
+    own.start()
+    for j in range(1, at.ny):
+        low_y_in(j).wait_recv()
+        low_core(j, True).start()
+    own.wait()
+    for j in range(at.ny):
+        low_core(j, False).wait_recv()
+        low_core(j, True).wait_send()
+    for j in range(1, at.ny):
+        low_y(j).wait_send()
+
+    def drain(i, _):
+        for j in range(at.ny):
+            core_copy(i, j).wait_send()
+        for j in range(1, at.ny):
+            y_copy(i, j).wait_send()
+        return 0
+
+    def drain_home(i, _):
+        home_copy(i).wait_send()
+        return 0
+
+    lax.fori_loop(0, n_sp, drain, 0)
+    lax.fori_loop(0, n_sp - 1, drain_home, 0)
+
+
+def give_back(part, pick, cot, n_sp, n_tp):
+    total, width = part.shape
+    rows, cols, ny, tok = total // n_sp, width // n_tp, n_tp // CORES, cot.shape[0]
+    dma = pltpu.SemaphoreType.DMA
+    bf = jnp.bfloat16
+    return pl.pallas_call(
+        functools.partial(return_kernel, n_sp, n_tp),
+        out_shape=jax.ShapeDtypeStruct((tok, width), bf),
+        in_specs=[pl.BlockSpec(memory_space=pltpu.VMEM)] * 3,
+        out_specs=pl.BlockSpec(memory_space=pltpu.VMEM),
+        scratch_shapes=[
+            pltpu.VMEM((n_sp, ny, rows, cols), bf),
+            pltpu.VMEM((n_sp, rows, cols), jnp.float32),
+            pltpu.VMEM((n_sp, ny, rows, cols), bf),
+            pltpu.VMEM((n_sp, ny, rows, cols), bf),
+            pltpu.VMEM((n_sp, rows, cols), bf),
+            pltpu.VMEM((n_sp * rows, cols), bf),
+            pltpu.VMEM((tok, cols), bf),
+            dma((n_sp, ny)),
+            dma((n_sp, ny)),
+            dma((n_sp, ny)),
+            dma((n_sp, ny)),
+            dma((n_sp,)),
+            dma((n_sp,)),
+            dma((ny,)),
+            dma((ny,)),
+            dma((ny,)),
+            dma((ny,)),
+            dma,
+        ],
+        compiler_params=pltpu.CompilerParams(
+            collective_id=1, has_side_effects=True, vmem_limit_bytes=VMEM_LIMIT
+        ),
+    )(part, pick, cot)
+
+
+def close_kernel(n_sp, n_tp, part, link, proj, carry, held, links, sg, rg, sk, rk):
+    at = Place(n_sp, n_tp)
+    rows = part.shape[0] // n_sp
+
+    def proj_copy(i):
+        peer = at.sp_peer(i)
+        return remote(
+            part.at[pl.ds(aligned(peer, rows), rows), :],
+            held.at[i],
+            sg.at[i],
+            rg.at[i],
+            (peer, at.t),
+        )
+
+    def link_copy(i):
+        return remote(link, links.at[i], sk.at[i], rk.at[i], (at.sp_peer(i), at.t))
+
+    at.barrier(False)
+
+    def send_link(i, _):
+        link_copy(i).start()
+        return 0
+
+    def send_proj(i, _):
+        proj_copy(i).start()
+        return 0
+
+    lax.fori_loop(1, n_sp, send_link, 0)
+    lax.fori_loop(1, n_sp, send_proj, 0)
+
+    def compose(k, state):
+        i = k + 1
+        link_copy(i).wait_recv()
+        ahead = n_sp - i
+        later = at.s + ahead < n_sp
+        lower = links[i]
+        return jnp.where(later, lower[0:1] * state + lower[1:2], state)
+
+    carry[...] = lax.fori_loop(0, n_sp - 1, compose, jnp.zeros(carry.shape, jnp.float32))
+
+    proj[...] = part[pl.ds(aligned(at.s, rows), rows), :].astype(jnp.float32)
+
+    def add(i, _):
+        proj_copy(i).wait_recv()
+        proj[...] += held[i].astype(jnp.float32)
+        return 0
+
+    lax.fori_loop(1, n_sp, add, 0)
+
+    def drain(i, _):
+        link_copy(i).wait_send()
+        proj_copy(i).wait_send()
+        return 0
+
+    lax.fori_loop(1, n_sp, drain, 0)
+
+
+def close(part, link, n_sp, n_tp):
+    total, channels = part.shape
+    dma = pltpu.SemaphoreType.DMA
+    return pl.pallas_call(
+        functools.partial(close_kernel, n_sp, n_tp),
+        out_shape=(
+            jax.ShapeDtypeStruct((total // n_sp, channels), jnp.float32),
+            jax.ShapeDtypeStruct((1, channels), jnp.float32),
+        ),
+        in_specs=[pl.BlockSpec(memory_space=pltpu.VMEM)] * 2,
+        out_specs=[pl.BlockSpec(memory_space=pltpu.VMEM)] * 2,
+        scratch_shapes=[
+            pltpu.VMEM((n_sp, total // n_sp, channels), jnp.bfloat16),
+            pltpu.VMEM((n_sp,) + link.shape, jnp.float32),
+            dma((n_sp,)),
+            dma((n_sp,)),
+            dma((n_sp,)),
+            dma((n_sp,)),
+        ],
+        compiler_params=pltpu.CompilerParams(
+            collective_id=2, has_side_effects=True, vmem_limit_bytes=VMEM_LIMIT
+        ),
+    )(part, link)
 
 
 def local(
@@ -63,32 +490,41 @@
     decay_param,
     decay_shift,
 ):
-    sp_count = lax.axis_size("sp")
+    sp_count, tp_count = lax.axis_size("sp"), lax.axis_size("tp")
     tok_rows, model_width = cotangent.shape
     top_count = route_ids.shape[1]
     local_experts = w_gate.shape[0]
     expert_count = local_experts * sp_count
     capacity = 2 * tok_rows * top_count // expert_count
+    slots = expert_count * capacity
+    share_cols = model_width // tp_count
     flat_ids = route_ids.reshape(-1)
-    onehot = (flat_ids[:, None] == jnp.arange(expert_count, dtype=jnp.int32)[None, :]).astype(
-        jnp.int32
-    )
-    slot_index = jnp.sum((jnp.cumsum(onehot, axis=0) - onehot) * onehot, axis=1)
-    target = flat_ids * capacity + slot_index
-    scaled = (route_weights[:, :, None] * cotangent[:, None, :].astype(jnp.float32)).astype(
-        jnp.bfloat16
-    )
-    scaled = scaled.reshape(-1, model_width)
-    copies = jnp.broadcast_to(stream[:, None, :], (tok_rows, top_count, model_width)).reshape(
-        -1, model_width
-    )
-    empty_rows = jnp.zeros((expert_count * capacity, model_width), jnp.bfloat16)
-    rows_sent = empty_rows.at[target].set(scaled)
-    tokens_sent = empty_rows.at[target].set(copies)
-    grads_in, tokens_in = (
-        lax.all_to_all(rows_sent, "sp", split_axis=0, concat_axis=0, tiled=True),
-        lax.all_to_all(tokens_sent, "sp", split_axis=0, concat_axis=0, tiled=True),
-    )
+    pair_at = jnp.arange(flat_ids.shape[0], dtype=jnp.int32)
+    earlier = (flat_ids[:, None] == flat_ids[None, :]) & (pair_at[None, :] < pair_at[:, None])
+    slot_index = jnp.sum(earlier.astype(jnp.int32), axis=1)
+    target = (flat_ids * capacity + slot_index).reshape(tok_rows, top_count)
+    slot_at = jnp.arange(slots, dtype=jnp.int32)
+    lands = [target[:, k][None, :] == slot_at[:, None] for k in range(top_count)]
+    lands_any = functools.reduce(jnp.logical_or, lands)
+    pick = functools.reduce(
+        jnp.logical_or, [target[:, k][:, None] == slot_at[None, :] for k in range(top_count)]
+    ).astype(jnp.bfloat16)
+    first_col = lax.axis_index("tp") * share_cols
+    own_stream = lax.dynamic_slice_in_dim(stream, first_col, share_cols, 1)
+    own_cot = lax.dynamic_slice_in_dim(cotangent, first_col, share_cols, 1)
+    scaled = [
+        (route_weights[:, k : k + 1] * own_cot.astype(jnp.float32)).astype(jnp.bfloat16)
+        for k in range(top_count)
+    ]
+    tok_src = jnp.dot(
+        lands_any.astype(jnp.bfloat16), own_stream, preferred_element_type=jnp.float32
+    ).astype(jnp.bfloat16)
+    grd_src = jnp.dot(
+        jnp.concatenate(lands, axis=1).astype(jnp.bfloat16),
+        jnp.concatenate(scaled, axis=0),
+        preferred_element_type=jnp.float32,
+    ).astype(jnp.bfloat16)
+    tokens_in, grads_in = dispatch(tok_src, grd_src, sp_count, tp_count)
     grads_in = grads_in.reshape(sp_count, local_experts, capacity, model_width)
     tokens_in = tokens_in.reshape(sp_count, local_experts, capacity, model_width)
     gate_pre = jnp.einsum("secd,edf->secf", tokens_in, w_gate, preferred_element_type=jnp.float32)
@@ -104,28 +540,14 @@
     partial_value = partial_value + jnp.einsum(
         "secf,edf->secd", d_up, w_up, preferred_element_type=jnp.float32
     )
-    share = lax.psum_scatter(
-        partial_value.astype(jnp.bfloat16), "tp", scatter_dimension=3, tiled=True
-    )
-    share_cols = share.shape[3]
-    returned = lax.all_to_all(
-        share.reshape(-1, share_cols), "sp", split_axis=0, concat_axis=0, tiled=True
-    )
-    per_pair = returned[target].astype(jnp.float32).reshape(tok_rows, top_count, share_cols)
-    own_cols = lax.dynamic_slice_in_dim(cotangent, lax.axis_index("tp") * share_cols, share_cols, 1)
-    share_low = (own_cols.astype(jnp.float32) + jnp.sum(per_pair, axis=1)).astype(jnp.bfloat16)
-    stream_low = lax.all_gather(share_low, "tp", axis=1, tiled=True)
+    partial_low = partial_value.astype(jnp.bfloat16).reshape(slots, model_width)
+    stream_low = give_back(partial_low, pick, cotangent, sp_count, tp_count)
     d_mixed = lax.dot_general(
         out_proj, stream_low, (((0,), (1,)), ((), ())), preferred_element_type=jnp.float32
     )
-    grad_proj = lax.psum_scatter(
-        lax.dot_general(
-            stream_low, mixed, (((0,), (1,)), ((), ())), preferred_element_type=jnp.float32
-        ).astype(jnp.bfloat16),
-        "sp",
-        scatter_dimension=0,
-        tiled=True,
-    ).astype(jnp.float32)
+    proj_part = lax.dot_general(
+        stream_low, mixed, (((0,), (1,)), ((), ())), preferred_element_type=jnp.float32
+    ).astype(jnp.bfloat16)
     channels, positions = rec_input.shape
     gate_heads = rec_gates.shape[0]
     head_dim = rec_gates.shape[1]
@@ -157,9 +579,11 @@
     tail_decay = jnp.exp(total_log - log_cumsum)
     device_prod = jnp.exp(total_log[:, 0])
     head_term = decay_rate[:, 0] * local_adj[:, 0]
-    identity = (jnp.ones((channels,), jnp.float32), jnp.zeros((channels,), jnp.float32))
-    carried = carried_in((device_prod, head_term), "sp", compose_maps, identity)
-    adjoint = local_adj + tail_decay * carried[1][:, None]
+    link = jnp.concatenate(
+        [device_prod[None], head_term[None], jnp.zeros((6, channels), jnp.float32)], axis=0
+    )
+    grad_proj, carried = close(proj_part, link, sp_count, tp_count)
+    adjoint = local_adj + tail_decay * carried[0][:, None]
     mult_term = adjoint * in_gate * rec_value * decay_rate * decay_rate / raw_mult
     d_log = adjoint * state_before * decay_rate - jnp.where(at_start, 0.0, mult_term)
     d_rec_pre = (d_log * -RATE_SCALE * soft_plus * rec_gate * (1.0 - rec_gate)).astype(jnp.bfloat16)

time: 269 us -> 142 us (0.53)
  waiting for transfers between devices: 126 us -> 0 us
  Pallas kernels: 0 us -> 99.1 us
  blocking collectives: 42 us -> 0 us
  starting transfers between devices: 17.5 us -> 0 us
  local copies, waits for them, and re-layouts: 23.5 us -> 7.82 us
  between operations: 14.8 us -> 1.38 us
  matrix products: 34.4 us -> 27.7 us
  other arithmetic: 9.23 us -> 4.6 us
    pallas_call x0 -> x3, Pallas kernels: none -> 99.1 us  [the longest x1 44.7 us: dispatch(): pl.pallas_call(functools.partial(dispatch_kernel, n_sp, n_tp), out_shape=...]
    all_to_all x3 -> x0, waiting for transfers between devices: 82 us -> none  [the longest x1 39.3 us: local(): lax.all_to_all(rows_sent, 'sp', split_axis=0, concat_axis=0, tiled=True)]
    reduce_scatter x2 -> x0, waiting for transfers between devices: 44.4 us -> none  [the longest x1 23.4 us: local(): lax.psum_scatter(lax.dot_general(stream_low, mixed, (((0,), (1,)), ((), (...]
    all_gather x3 -> x0, blocking collectives: 42 us -> none  [the longest x2 35.3 us: carried_in(): gathered = jax.tree.map(lambda a: lax.all_gather(a, axis), part)]
    all_to_all x3 -> x0, starting transfers between devices: 17.3 us -> none  [the longest x1 7.41 us: local(): lax.all_to_all(tokens_sent, 'sp', split_axis=0, concat_axis=0, tiled=True)]
    mul x5 -> x1, local copies, waits for them, and re-layouts: 6.42 us -> 0.76 us  [local(): route_weights[:, k:k + 1] * own_cot.astype(jnp.float32)]
    scatter x1 -> x0, other arithmetic: 4.83 us -> none  [local(): rows_sent = empty_rows.at[target].set(scaled)]
    scatter x1 -> x0, local copies, waits for them, and re-layouts: 4.4 us -> none  [local(): tokens_sent = empty_rows.at[target].set(copies)]
  transfers between devices with their start and end apart: 5 -> 0, of which waited for: 5 -> 0; matrix products, arithmetic and copies ran while one was open for 15% -> 0% of each run, Pallas kernels for 0% -> 0%
where the time goes in v1:
time: 142 us; the launch traced here: 141 us
  Pallas kernels  99.1 us (70%)
  matrix products  27.7 us (20%)
  local copies, waits for them, and re-layouts  7.82 us (6%)
  other arithmetic  4.6 us (3%)
    pallas_call x1, Pallas kernels, dispatch(): pl.pallas_call(functools.partial(dispatch_kernel, n_sp, n_tp), out_shape=...  44.7 us
    pallas_call x1, Pallas kernels, give_back(): pl.pallas_call(functools.partial(return_kernel, n_sp, n_tp), out_shape=ja...  38.1 us
    pallas_call x1, Pallas kernels, close(): pl.pallas_call(functools.partial(close_kernel, n_sp, n_tp), out_shape=(ja...  16.3 us
    unnamed x44, local copies, waits for them, and re-layouts  5.39 us
    dot_general x1, matrix products, local(): jnp.einsum('secd,edf->secf', tokens_in, w_up, preferred_element_type=jnp....  3.62 us

profile of v1, /device:TPU:0, one launch (start us, length us, event | category | flops | bytes accessed | tf_op | source)
XLA Modules:
  0.0 140.7 jit_solution(10821257031394721438)
XLA Ops:
  0.7 0.9 copy.111
  1.7 0.2 convert_reduce_fusion
  2.1 0.7 multiply_add_fusion.11
  2.8 2.0 %convolution_convert_fusion.2.tok_src = bf16[512,512]{1,0:T(8,128)(2,1)} fusion(bf16[128,2048]{1,0:T(8,128)(2,1)} %param.16, s32[]{:T(128)S(6)} %select_n.66, s32[128]{0:T(128)S(1)} %get-tuple-element.75, s32[128]{0:T(128)S(1)} %get-tuple-element.74), kind=kOutput, calls=%fused_computation.20 | convolution fusion | flops 67567616 | bytes 656388 | tf_op jit(solution)/shard_map/dot_general | solution.py:519
  4.9 0.8 slice_bitcast_fusion.1
  5.7 1.0 fusion.44
  6.7 1.1 convolution_convert_fusion.1.grd_src
  7.8 44.7 %shard_map.199 = (bf16[512,2048]{1,0:T(8,128)(2,1)}, bf16[512,2048]{1,0:T(8,128)(2,1)}) custom-call(bf16[512,512]{1,0:T(8,128)(2,1)} %convolution_convert_fusion.2.tok_src, bf16[512,512]{1,0:T(8,128)(2,1)} %convolution_convert_fusion.1.grd_src), custom_call_target="tpu_custom_call" | custom-call | tf_op jit(solution)/shard_map/pallas_call | solution.py:194
  52.5 3.6 %fusion.8 = f32[8,64,512]{2,1,0:T(8,128)S(1)} fusion(bf16[8,64,2048]{2,1,0:T(8,128)(2,1)} %bitcast.183, bf16[1,2048,512]{2,1,0:T(8,128)(2,1)} %param.21), kind=kOutput, calls=%fused_computation.13 | convolution fusion | flops 1073741824 | bytes 5242880 | tf_op jit(solution)/shard_map/secd,edf->secf/dot_general | solution.py:531
  56.2 1.3 fusion.5
  57.4 0.3 copy-done.14
  57.7 0.6 copy-done.15
  58.4 2.3 %fusion.26 = (bf16[8,1,64,512]{3,2,0,1:T(8,128)(2,1)S(1)}, bf16[8,1,64,512]{3,2,0,1:T(8,128)(2,1)S(1)}) fusion(f32[8,64,512]{2,1,0:T(8,128)S(1)} %fusion.8, f32[8,64,512]{2,1,0:T(8,128)S(1)} %fusion.5, bf16[8,64,2048]{2,1,0:T(8,128)(2,1)S(1)} %bitcast.181, bf16[1,512,2048]{2,1,0:T(8,128)(2,1)S(1)} %copy-done.14), kind=kOutput, calls=%fused_computation.37 | convolution fusion | flops 1082916864 | bytes 7340032 | tf_op jit(solution)/shard_map/secd,efd->secf/dot_general | solution.py:534
  60.6 2.6 %fusion = bf16[1,2048,512]{2,1,0:T(8,128)(2,1)} fusion(bf16[8,64,2048]{2,1,0:T(8,128)(2,1)S(1)} %bitcast.185, bf16[8,1,64,512]{3,2,0,1:T(8,128)(2,1)S(1)} %get-tuple-element.49), kind=kOutput, calls=%fused_computation.4 | convolution fusion | flops 1074790400 | bytes 4718592 | tf_op jit(solution)/shard_map/secd,secf->edf/dot_general | solution.py:29
  63.3 2.6 %fusion.1 = bf16[1,2048,512]{2,1,0:T(8,128)(2,1)} fusion(bf16[8,64,2048]{2,1,0:T(8,128)(2,1)S(1)} %bitcast.186, bf16[8,1,64,512]{3,2,0,1:T(8,128)(2,1)S(1)} %get-tuple-element.48), kind=kOutput, calls=%fused_computation.5 | convolution fusion | flops 1074790400 | bytes 4718592 | tf_op jit(solution)/shard_map/secd,secf->edf/dot_general | solution.py:30
  65.9 2.8 %fusion.2 = bf16[1,512,2048]{2,1,0:T(8,128)(2,1)} fusion(bf16[8,64,2048]{2,1,0:T(8,128)(2,1)S(1)} %bitcast.182, f32[8,64,512]{2,1,0:T(8,128)S(1)} %fusion.8, f32[8,64,512]{2,1,0:T(8,128)S(1)} %fusion.5), kind=kOutput, calls=%fused_computation.6 | convolution fusion | flops 1077411840 | bytes 6291456 | tf_op jit(solution)/shard_map/secf,secd->efd/dot_general | solution.py:31
  68.7 1.3 fusion.3
  70.0 0.3 copy-done.2
  70.3 2.6 %add_convert_fusion = bf16[8,64,2048]{2,1,0:T(8,128)(2,1)} fusion(f32[8,64,2048]{2,1,0:T(8,128)S(1)} %fusion.3, bf16[1,2048,512]{2,1,0:T(8,128)(2,1)S(1)} %copy-done.2, bf16[8,1,64,512]{3,2,0,1:T(8,128)(2,1)S(1)} %get-tuple-element.48), kind=kOutput, calls=%fused_computation.3 | convolution fusion | flops 1075838976 | bytes 8912896 | tf_op jit(solution)/shard_map/secf,edf->secd/dot_general | solution.py:540
  72.9 0.8 fusion.51.pick
  73.7 38.1 %shard_map.200 = bf16[128,2048]{1,0:T(8,128)(2,1)} custom-call(bf16[512,2048]{1,0:T(8,128)(2,1)} %bitcast.172, bf16[128,512]{1,0:T(8,128)(2,1)} %fusion.51.pick, bf16[128,2048]{1,0:T(8,128)(2,1)} %cot.1), custom_call_target="tpu_custom_call" | custom-call | tf_op jit(solution)/shard_map/pallas_call | solution.py:362
  111.8 2.3 %convolution_convert_fusion.part = bf16[2048,128]{1,0:T(8,128)(2,1)} fusion(bf16[128,2048]{1,0:T(8,128)(2,1)} %shard_map.200, bf16[128,128]{1,0:T(8,128)(2,1)S(1)} %copy-done.8), kind=kOutput, calls=%fused_computation.7 | convolution fusion | flops 67371008 | bytes 1081344 | tf_op jit(solution)/shard_map/dot_general | solution.py:548
  114.4 1.0 fusion.17
  115.6 0.7 copy.115
  116.3 0.2 fusion.20
  116.7 1.8 %fusion.56 = (f32[128,128]{0,1:T(8,128)}, f32[128,128]{0,1:T(8,128)S(1)}, f32[128,128]{0,1:T(8,128)S(1)}) fusion(bf16[128,128]{0,1:T(8,128)(2,1)S(1)} %copy.116, bf16[128,128]{0,1:T(8,128)(2,1)S(1)} %copy.121, f32[128,128]{0,1:T(8,128)S(1)} %copy.118, f32[128,128]{0,1:T(8,128)S(1)} %copy.119, pred[128]{0:T(512)(128)(4,1)S(1)} %add_compare_fusion, ...), kind=kOutput, calls=%fused_computation.90 | convolution fusion | flops 67649536 | bytes 1573504 | tf_op jit(solution)/shard_map/dot_general | solution.py:545
  120.1 0.7 maximum_maximum_fusion.link
  120.7 16.3 %shard_map.201 = (f32[256,128]{1,0:T(8,128)}, f32[1,128]{1,0:T(1,128)}) custom-call(bf16[2048,128]{1,0:T(8,128)(2,1)} %convolution_convert_fusion.part, f32[8,128]{1,0:T(8,128)} %maximum_maximum_fusion.link), custom_call_target="tpu_custom_call" | custom-call | tf_op jit(solution)/shard_map/pallas_call | solution.py:453
  137.1 0.8 fusion.59
  138.5 0.7 copy.131
  139.3 0.7 copy.132
  140.0 0.7 copy.140
  (143 shorter events, 2.8 us)
Async XLA Ops:
  0.6 55.5 %copy-start = (bf16[1,2048,512]{2,1,0:T(8,128)(2,1)S(1)}, bf16[1,2048,512]{2,1,0:T(8,128)(2,1)}, u32[]{:S(2)}) copy-start(bf16[1,2048,512]{2,1,0:T(8,128)(2,1)} %param.20) | copy-start | bytes 6291460
  52.5 3.6 %copy-start.16 = (bf16[512,2048]{1,0:T(8,128)(2,1)S(1)}, bf16[512,2048]{1,0:T(8,128)(2,1)}, u32[]{:S(2)}) copy-start(bf16[512,2048]{1,0:T(8,128)(2,1)} %get-tuple-element.10) | copy-start | bytes 6291460
  56.1 1.6 %copy-start.14 = (bf16[1,512,2048]{2,1,0:T(8,128)(2,1)S(1)}, bf16[1,512,2048]{2,1,0:T(8,128)(2,1)}, u32[]{:S(2)}) copy-start(bf16[1,512,2048]{2,1,0:T(8,128)(2,1)} %param.22) | copy-start | bytes 6291460
  56.2 2.2 %copy-start.15 = (bf16[512,2048]{1,0:T(8,128)(2,1)S(1)}, bf16[512,2048]{1,0:T(8,128)(2,1)}, u32[]{:S(2)}) copy-start(bf16[512,2048]{1,0:T(8,128)(2,1)} %get-tuple-element.11) | copy-start | bytes 6291460
  68.7 1.6 %copy-start.2 = (bf16[1,2048,512]{2,1,0:T(8,128)(2,1)S(1)}, bf16[1,2048,512]{2,1,0:T(8,128)(2,1)}, u32[]{:S(2)}) copy-start(bf16[1,2048,512]{2,1,0:T(8,128)(2,1)} %param.21) | copy-start | bytes 6291460
  72.9 38.9 %copy-start.8 = (bf16[128,128]{1,0:T(8,128)(2,1)S(1)}, bf16[128,128]{1,0:T(8,128)(2,1)}, u32[]{:S(2)}) copy-start(bf16[128,128]{1,0:T(8,128)(2,1)} %param.24) | copy-start | bytes 98308
  73.7 40.4 %copy-start.9 = (bf16[128,128]{1,0:T(8,128)(2,1)S(1)}, bf16[128,128]{1,0:T(8,128)(2,1)}, u32[]{:S(2)}) copy-start(bf16[128,128]{1,0:T(8,128)(2,1)} %param.26) | copy-start | bytes 98308
  73.7 40.6 %copy-start.10 = (bf16[128,128]{1,0:T(8,128)(2,1)S(1)}, bf16[128,128]{1,0:T(8,128)(2,1)}, u32[]{:S(2)}) copy-start(bf16[128,128]{1,0:T(8,128)(2,1)} %param.25) | copy-start | bytes 98308
  73.7 41.8 %copy-start.6 = (f32[128,128]{1,0:T(8,128)S(1)}, f32[128,128]{1,0:T(8,128)}, u32[]{:S(2)}) copy-start(f32[128,128]{1,0:T(8,128)} %param.27) | copy-start | bytes 196612
  73.7 41.9 %copy-start.7 = (f32[128,128]{1,0:T(8,128)S(1)}, f32[128,128]{1,0:T(8,128)}, u32[]{:S(2)}) copy-start(f32[128,128]{1,0:T(8,128)} %param.31) | copy-start | bytes 196612
  73.7 42.6 %copy-start.11 = (bf16[4,32,32]{2,1,0:T(8,128)(2,1)S(1)}, bf16[4,32,32]{2,1,0:T(8,128)(2,1)}, u32[]{:S(2)}) copy-start(bf16[4,32,32]{2,1,0:T(8,128)(2,1)} %param.28) | copy-start | bytes 24580
  73.7 42.9 %copy-start.17 = (f32[128]{0:T(128)S(1)}, f32[128]{0:T(128)}, u32[]{:S(2)}) copy-start(f32[128]{0:T(128)} %param.30) | copy-start | bytes 1540
  73.7 42.9 %copy-start.3 = (bf16[2048,128]{1,0:T(8,128)(2,1)S(1)}, bf16[2048,128]{1,0:T(8,128)(2,1)}, u32[]{:S(2)}) copy-start(bf16[2048,128]{1,0:T(8,128)(2,1)} %param.23) | copy-start | bytes 1572868
  111.8 4.8 %copy-start.1 = (bf16[128,2048]{1,0:T(8,128)(2,1)S(1)}, bf16[128,2048]{1,0:T(8,128)(2,1)}, u32[]{:S(2)}) copy-start(bf16[128,2048]{1,0:T(8,128)(2,1)} %shard_map.200) | copy-start | bytes 1572868
  118.5 19.5 %copy-start.12 = (bf16[4,32,32]{2,1,0:T(8,128)(2,1)S(1)}, bf16[4,32,32]{2,1,0:T(8,128)(2,1)}, u32[]{:S(2)}) copy-start(bf16[4,32,32]{2,1,0:T(8,128)(2,1)} %param.28) | copy-start | bytes 24580
  118.6 19.7 %copy-start.13 = (bf16[4,32,32]{2,1,0:T(8,128)(2,1)S(1)}, bf16[4,32,32]{2,1,0:T(8,128)(2,1)}, u32[]{:S(2)}) copy-start(bf16[4,32,32]{2,1,0:T(8,128)(2,1)} %param.29) | copy-start | bytes 24580
  118.8 20.5 %copy-start.4 = (f32[128,128]{0,1:T(8,128)S(1)}, f32[128,128]{0,1:T(8,128)}, u32[]{:S(2)}) copy-start(f32[128,128]{0,1:T(8,128)} %get-tuple-element.44) | copy-start | bytes 196612
  137.1 2.9 %copy-start.5 = (f32[256,128]{1,0:T(8,128)S(1)}, f32[256,128]{1,0:T(8,128)}, u32[]{:S(2)}) copy-start(f32[256,128]{1,0:T(8,128)} %get-tuple-element.87) | copy-start | bytes 393220
